TPU v7x, 32 devices: a whole 2x2x4 slice. The times are simulated.
32 devices in a mesh: sp: 8 (over z, y), tp: 4 (over x, core).
Axes of the slice: x: 2, y: 2, z: 4, core: 2. Of those that a mesh axis runs over, the one named last changes fastest.
Arguments:
- resid: bfloat16 [6144, 2048], P(('sp', 'tp')), may hold values from -6 to 6
- query: bfloat16 [6144, 1024], P('sp', 'tp'), may hold values from -6 to 6
- keys: bfloat16 [6144, 1024], P('sp', 'tp'), may hold values from -6 to 6
- values: bfloat16 [6144, 1024], P('sp', 'tp'), may hold values from -6 to 6
- out_gate: bfloat16 [6144, 1024], P(('sp', 'tp')), may hold values from -6 to 6
- forget_pre: float32 [4, 6144], P('tp', 'sp'), may hold values from 0 to 16
- input_pre: float32 [4, 6144], P('tp', 'sp'), may hold values from -4 to 130
- head_gain: float32 [1024], replicated, may hold values from 0.1 to 1.9
- out_proj: bfloat16 [1024, 2048], replicated, may hold values from -0.1875 to 0.1875
- ffn_gain: float32 [2048], replicated, may hold values from 0.1 to 1.9
- routes: int32 [6144, 2], P(('sp', 'tp')), may hold values from 0 to 7, all different within a row; in each aligned block of 96 rows (0 to 95, 96 to 191, ...) at most 48 rows name the same one
- route_scores: float32 [6144, 2], P(('sp', 'tp')), may hold values from 0.1 to 1
- w_gate: bfloat16 [8, 2048, 512], P('sp'), may hold values from -0.125 to 0.125
- w_up: bfloat16 [8, 2048, 512], P('sp'), may hold values from -0.125 to 0.125
- w_down: bfloat16 [8, 512, 2048], P('sp'), may hold values from -0.25 to 0.25
Outputs:
- layer_out: bfloat16 [6144, 2048], P(('sp', 'tp'))
Inputs may be any that keep to these rules, and one draw needn't show every extreme that they name: `routes`: each row names 2 different experts; in each aligned block of 96 rows no expert is named by more than 48 rows, a bound that some block reaches.
All inputs are finite; a program needn't handle non-finite values.
Results may differ from a plain program's by a relative error of at most 0.0095.
Values may be sent and summed in bfloat16 or wider, within the bound.
A program may use at most 128 MiB of HBM per device.

v0:
```python
import jax
import jax.numpy as jnp
from jax import lax
from jax.sharding import PartitionSpec as P

BLOCK = 64
EPS = 1e-06
FLOOR_LOG = -1e30
HIGHEST = lax.Precision.HIGHEST


def prefix(part, axis, combine, identity):
    place = lax.axis_index(axis)
    gathered = jax.tree.map(lambda a: lax.all_gather(a, axis), part)
    state = jax.tree.map(lambda a, e: jnp.zeros_like(a) + jnp.asarray(e, a.dtype), part, identity)

    def one(step, state):
        return combine(
            state, jax.tree.map(lambda a: lax.dynamic_index_in_dim(a, step, 0, False), gathered)
        )

    return lax.fori_loop(0, place, one, state)


def block_pass(query, keys, values, log_forget, log_input, state):
    seq_len, head_width = query.shape
    blocks = seq_len // BLOCK
    key_scale = head_width ** (-0.5)
    causal = jnp.tril(jnp.ones((BLOCK, BLOCK), dtype=bool))

    def block_step(state_in, inputs):
        state_mat, state_vec, max_log = state_in
        q_block, k_block, v_block, forget_blk, input_blk = inputs
        cum_log = jnp.cumsum(forget_blk)
        block_total = cum_log[-1]
        log_mat = jnp.where(
            causal, cum_log[:, None] - cum_log[None, :] + input_blk[None, :], -jnp.inf
        )
        inter_log = cum_log + max_log
        row_max = jnp.maximum(inter_log, jnp.max(log_mat, axis=1))
        weight_mat = jnp.exp(log_mat - row_max[:, None])
        carry_weight = jnp.exp(inter_log - row_max)
        scores = jnp.dot(q_block, k_block.T, preferred_element_type=jnp.float32) * key_scale
        weights_blk = (scores * weight_mat).astype(jnp.bfloat16)
        q_float = q_block.astype(jnp.float32)
        numerator = carry_weight[:, None] * jnp.dot(
            q_float, state_mat, precision=HIGHEST
        ) + jnp.dot(weights_blk, v_block, preferred_element_type=jnp.float32)
        denominator = carry_weight * jnp.dot(q_float, state_vec, precision=HIGHEST) + jnp.sum(
            weights_blk.astype(jnp.float32), axis=1
        )
        log_keep = block_total - cum_log + input_blk
        new_max = jnp.maximum(block_total + max_log, jnp.max(log_keep))
        keep_weight = jnp.exp(log_keep - new_max)
        decay_now = jnp.exp(block_total + max_log - new_max)
        k_float = k_block.astype(jnp.float32) * key_scale
        state_mat = decay_now * state_mat + jnp.dot(
            (k_float * keep_weight[:, None]).T, v_block.astype(jnp.float32), precision=HIGHEST
        )
        state_vec = decay_now * state_vec + jnp.dot(keep_weight, k_float, precision=HIGHEST)
        return ((state_mat, state_vec, new_max), (numerator, denominator, row_max))

    def to_blocks(array_in):
        return array_in.reshape((blocks, BLOCK) + array_in.shape[1:])

    ignored, outputs = lax.scan(
        block_step,
        state,
        (
            to_blocks(query),
            to_blocks(keys),
            to_blocks(values),
            to_blocks(log_forget),
            to_blocks(log_input),
        ),
    )
    numerator, denominator, row_max = outputs
    return (
        numerator.reshape(seq_len, head_width),
        denominator.reshape(seq_len),
        row_max.reshape(seq_len),
    )


def end_state(keys, values, log_forget, log_input):
    head_width = keys.shape[1]
    cum_log = jnp.cumsum(log_forget)
    block_total = cum_log[-1]
    log_keep = block_total - cum_log + log_input
    max_log = jnp.max(log_keep)
    keep_weight = jnp.exp(log_keep - max_log)
    k_float = keys.astype(jnp.float32) * head_width ** (-0.5)
    state_mat = jnp.dot(
        (k_float * keep_weight[:, None]).T, values.astype(jnp.float32), precision=HIGHEST
    )
    state_vec = jnp.dot(keep_weight, k_float, precision=HIGHEST)
    return (state_mat, state_vec, max_log, block_total)


def join_states(earlier, latter):
    old_mat, old_vec, old_max, old_total = earlier
    new_mat, new_vec, new_max, new_total = latter
    joined_max = jnp.maximum(new_total + old_max, new_max)
    keep_old = jnp.exp(new_total + old_max - joined_max)
    keep_new = jnp.exp(new_max - joined_max)
    joined_mat = keep_old[:, None, None] * old_mat + keep_new[:, None, None] * new_mat
    joined_vec = keep_old[:, None] * old_vec + keep_new[:, None] * new_vec
    return (joined_mat, joined_vec, joined_max, old_total + new_total)


def slot_select(expert_ids, expert_count, capacity):
    flat_ids = expert_ids.reshape(-1)
    one_hot = (flat_ids[:, None] == jnp.arange(expert_count, dtype=jnp.int32)[None, :]).astype(
        jnp.int32
    )
    slot_rank = jnp.sum((jnp.cumsum(one_hot, axis=0) - 1) * one_hot, axis=1)
    target = flat_ids * capacity + slot_rank
    return (
        jnp.arange(expert_count * capacity, dtype=jnp.int32)[:, None] == target[None, :]
    ).astype(jnp.bfloat16)


def run_experts(arrived, w_gate, w_up, w_down, sources):
    local_count = w_gate.shape[0]
    grouped = arrived.reshape(sources, local_count, arrived.shape[1], arrived.shape[2])
    gate_pre = jnp.einsum("pesd,edf->pesf", grouped, w_gate, preferred_element_type=jnp.float32)
    up_pre = jnp.einsum("pesd,edf->pesf", grouped, w_up, preferred_element_type=jnp.float32)
    active = (jax.nn.silu(gate_pre) * up_pre).astype(jnp.bfloat16)
    result = jnp.einsum(
        "pesf,efd->pesd", active, w_down, preferred_element_type=jnp.float32
    ).astype(jnp.bfloat16)
    return result.reshape(arrived.shape)


def shards(
    resid,
    query,
    keys,
    values,
    out_gate,
    forget_pre,
    input_pre,
    head_gain,
    out_proj,
    ffn_gain,
    routes,
    route_scores,
    w_gate,
    w_up,
    w_down,
):
    local_heads = forget_pre.shape[0]
    seq_len = query.shape[0]
    head_width = query.shape[1] // local_heads
    log_forget = jax.nn.log_sigmoid(forget_pre)
    q_heads = query.reshape(seq_len, local_heads, head_width)
    k_heads = keys.reshape(seq_len, local_heads, head_width)
    v_heads = values.reshape(seq_len, local_heads, head_width)
    state_mat, state_vec, max_log, totals = jax.vmap(end_state, in_axes=(1, 1, 0, 0))(
        k_heads, v_heads, log_forget, input_pre
    )
    identity = (
        jnp.zeros((local_heads, head_width, head_width), jnp.float32),
        jnp.zeros((local_heads, head_width), jnp.float32),
        jnp.full((local_heads,), FLOOR_LOG, jnp.float32),
        jnp.zeros((local_heads,), jnp.float32),
    )
    carried = prefix((state_mat, state_vec, max_log, totals), "sp", join_states, identity)
    pass_heads = jax.vmap(block_pass, in_axes=(1, 1, 1, 0, 0, 0), out_axes=(1, 1, 1))
    numerator, denominator, row_max = pass_heads(
        q_heads, k_heads, v_heads, log_forget, input_pre, (identity[0], identity[1], identity[2])
    )
    cum_all = jnp.cumsum(log_forget, axis=1).T + carried[2][None, :]
    joined_max = jnp.maximum(row_max, cum_all)
    keep_own = jnp.exp(row_max - joined_max)
    keep_far = jnp.exp(cum_all - joined_max)
    q_float = q_heads.astype(jnp.float32)
    numerator = keep_own[:, :, None] * numerator + keep_far[:, :, None] * jnp.einsum(
        "lhd,hde->lhe", q_float, carried[0], precision=HIGHEST
    )
    denominator = keep_own * denominator + keep_far * jnp.einsum(
        "lhd,hd->lh", q_float, carried[1], precision=HIGHEST
    )
    row_max = joined_max
    hidden = numerator / jnp.maximum(jnp.abs(denominator), jnp.exp(-row_max))[:, :, None]
    cell_rows = hidden.reshape(seq_len, local_heads * head_width).astype(jnp.bfloat16)
    token_rows = lax.all_to_all(cell_rows, "tp", split_axis=0, concat_axis=1, tiled=True)
    cell_float = token_rows.astype(jnp.float32)
    headed = (
        cell_float
        * lax.rsqrt(jnp.mean(cell_float * cell_float, axis=1, keepdims=True) + EPS)
        * head_gain[None, :]
    )
    gated_out = (headed * jax.nn.sigmoid(out_gate.astype(jnp.float32))).astype(jnp.bfloat16)
    after_mix = resid.astype(jnp.float32) + jnp.dot(
        gated_out, out_proj, preferred_element_type=jnp.float32
    )
    normed_rows = (
        after_mix
        * lax.rsqrt(jnp.mean(after_mix * after_mix, axis=1, keepdims=True) + EPS)
        * ffn_gain[None, :]
    ).astype(jnp.bfloat16)
    row_count = normed_rows.shape[0]
    half_rows = row_count // 2
    route_count = routes.shape[1]
    sources = lax.axis_size("sp")
    expert_count = w_gate.shape[0] * sources
    capacity = max(2, 2 * half_rows * route_count // expert_count)
    selects = [
        slot_select(
            routes[half_idx * half_rows : (half_idx + 1) * half_rows], expert_count, capacity
        )
        for half_idx in range(2)
    ]

    def pack_rows(half_idx):
        selection = (
            selects[half_idx].reshape(expert_count * capacity, half_rows, route_count).sum(axis=2)
        )
        packed = jnp.dot(
            selection,
            normed_rows[half_idx * half_rows : (half_idx + 1) * half_rows],
            preferred_element_type=jnp.float32,
        )
        return packed.astype(jnp.bfloat16).reshape(expert_count, capacity, normed_rows.shape[1])

    send_rows = jnp.concatenate([pack_rows(0), pack_rows(1)], axis=1)
    finished = run_experts(
        lax.all_to_all(send_rows, "sp", split_axis=0, concat_axis=0, tiled=True),
        w_gate,
        w_up,
        w_down,
        sources,
    )
    returned = lax.all_to_all(finished, "sp", split_axis=0, concat_axis=0, tiled=True)
    answers = [returned[:, :capacity], returned[:, capacity:]]
    route_weight = route_scores / jnp.sum(route_scores, axis=1, keepdims=True)
    pieces = []
    for half_idx in range(2):
        gathered = lax.dot_general(
            selects[half_idx],
            answers[half_idx].reshape(expert_count * capacity, -1),
            (((0,), (0,)), ((), ())),
            preferred_element_type=jnp.float32,
        )
        weights_half = route_weight[half_idx * half_rows : (half_idx + 1) * half_rows]
        pieces.append(
            jnp.sum(gathered.reshape(half_rows, route_count, -1) * weights_half[:, :, None], axis=1)
        )
    return (after_mix + jnp.concatenate(pieces, axis=0)).astype(jnp.bfloat16)


def solution(mesh):
    placed = (
        P(("sp", "tp"), None),
        P("sp", "tp"),
        P("sp", "tp"),
        P("sp", "tp"),
        P(("sp", "tp"), None),
        P("tp", "sp"),
        P("tp", "sp"),
        P(),
        P(),
        P(),
        P(("sp", "tp"), None),
        P(("sp", "tp"), None),
        P("sp", None, None),
        P("sp", None, None),
        P("sp", None, None),
    )
    return jax.shard_map(
        shards, mesh=mesh, in_specs=placed, out_specs=P(("sp", "tp"), None), check_vma=False
    )
```

profile of v0, /device:TPU:0, one launch (start us, length us, event | category | flops | bytes accessed | tf_op | source)
XLA Modules:
  0.0 429.5 jit_solution(1679653552651287913)
XLA Ops:
  8.8 2.0 fusion.111
  11.4 2.8 fusion.79
  18.5 136.7 %while.38 = (s32[]{:T(128)}, f32[1,256,256]{2,1,0:T(8,128)S(1)}, f32[1,256]{1,0:T(1,128)S(1)}, f32[1]{0:T(128)}, f32[12,1,64,256]{3,2,1,0:T(8,128)}, /*index=5*/...) while((s32[]{:T(128)}, f32[1,256,256]{2,1,0:T(8,128)S(1)}, ...), condition=%wide.region_5.6_spmd.clone, body=%wide.region_0.5_spmd.clone.sunk | while | flops 105678720 | bytes 1283846 | solution.py:66
  24.5 1.6 fusion.158
  28.3 1.6 convolution_add_fusion.4
  35.9 1.6 fusion.158
  47.3 1.6 fusion.158
  51.1 1.6 convolution_add_fusion.4
  58.7 1.6 fusion.158
  62.5 1.6 convolution_add_fusion.4
  73.8 1.6 convolution_add_fusion.4
  85.2 1.6 convolution_add_fusion.4
  96.6 1.6 convolution_add_fusion.4
  108.0 1.6 convolution_add_fusion.4
  115.6 1.6 fusion.158
  119.4 1.6 convolution_add_fusion.4
  130.8 1.6 convolution_add_fusion.4
  142.2 1.6 convolution_add_fusion.4
  153.6 1.6 convolution_add_fusion.4
  155.2 23.8 %all-reduce.4 = (f32[8]{0:T(128)}, f32[8]{0:T(128)}) all-reduce(f32[8]{0:T(128)S(1)} %bitcast_dynamic-update-slice_fusion, f32[8]{0:T(128)S(1)} %dynamic-update-slice.1), channel_id=1, replica_groups=mesh['sp'=8,'tp'=4] {'sp'}, use_global_device_ids=true, to_apply=%add.2 | all-reduce | flops 16 | bytes 128
  186.8 16.3 %all-gather.2 = f32[8,1,256]{2,1,0:T(1,128)S(1)} all-gather(f32[1,1,256]{2,1,0:T(1,128)S(1)} %convolution_bitcast_fusion.3), channel_id=3, replica_groups=mesh['sp'=8,'tp'=4] {'sp'}, dimensions={0}, use_global_device_ids=true | all-gather | bytes 9216 | tf_op jit(solution)/shard_map/all_gather | solution.py:14
  207.6 1.9 copy.46
  209.5 3.5 all-to-all-start
  213.4 6.9 %all-to-all-done = bf16[4,192,256]{2,1,0:T(8,128)(2,1)S(1)} async-done(((bf16[4,192,256]{2,1,0:T(8,128)(2,1)}), bf16[4,192,256]{2,1,0:T(8,128)(2,1)S(1)}, u32[]{:S(2)}, u32[]{:S(2)}) %all-to-all-start) | async-done | bytes 393248 | tf_op jit(solution)/shard_map/all_to_all | solution.py:187
  221.5 3.5 multiply_reduce_fusion
  227.1 103.0 %all_to_all.20 = bf16[8,96,2048]{2,1,0:T(8,128)(2,1)S(1)} all-to-all(bf16[8,96,2048]{2,1,0:T(8,128)(2,1)S(1)} %pad_maximum_fusion), channel_id=1, replica_groups=mesh['sp'=8,'tp'=4] {'sp'}, dimensions={0} | all-to-all | bytes 6291456 | tf_op jit(solution)/shard_map/all_to_all | solution.py:229
  330.1 1.7 copy-done.3
  331.8 3.0 fusion.60
  334.9 8.2 %convolution_convert_fusion = bf16[8,96,2048]{2,1,0:T(8,128)(2,1)} fusion(bf16[1,512,2048]{2,1,0:T(8,128)(2,1)S(1)} %copy-done, bf16[8,96,2048]{2,1,0:T(8,128)(2,1)} %copy-done.3, bf16[1,2048,512]{2,1,0:T(8,128)(2,1)} %param.32, f32[8,96,512]{2,1,0:T(8,128)} %fusion.60), kind=kOutput, calls=%fused_computation.78 | convolution fusion | flops 3225157632 | bytes 12058624 | tf_op jit(solution)/shard_map/pesf,efd->pesd/dot_general | solution.py:129
  343.0 4.5 %all-to-all-start.2 = ((bf16[8,96,2048]{2,1,0:T(8,128)(2,1)}), bf16[8,96,2048]{2,1,0:T(8,128)(2,1)}, u32[]{:S(2)}, u32[]{:S(2)}) async-start(bf16[8,96,2048]{2,1,0:T(8,128)(2,1)} %convolution_convert_fusion), calls=%async_computation.2 | async-start | bytes 6291456 | tf_op jit(solution)/shard_map/all_to_all | solution.py:235
  348.1 69.2 %all-to-all-done.2 = bf16[8,96,2048]{2,1,0:T(8,128)(2,1)} async-done(((bf16[8,96,2048]{2,1,0:T(8,128)(2,1)}), bf16[8,96,2048]{2,1,0:T(8,128)(2,1)}, u32[]{:S(2)}, u32[]{:S(2)}) %all-to-all-start.2) | async-done | bytes 3145760 | tf_op jit(solution)/shard_map/all_to_all | solution.py:235
  417.3 2.3 fusion.112
  (290 shorter events, 122.3 us)
Async XLA Ops:
  6.5 328.3 %copy-start = (bf16[1,512,2048]{2,1,0:T(8,128)(2,1)S(1)}, bf16[1,512,2048]{2,1,0:T(8,128)(2,1)}, u32[]{:S(2)}) copy-start(bf16[1,512,2048]{2,1,0:T(8,128)(2,1)} %param.33) | copy-start | bytes 6291460
  6.5 197.2 %all-gather.5.cloned.1.call-start = ((), (), s32[]{:S(2)}) async-start(), calls=%async_computation.3 | async-start | bytes 2359296 | tf_op jit(solution)/shard_map/all_gather | solution.py:14
  8.1 10.4 %copy-start.21 = (f32[6]{0:T(128)}, f32[6]{0:T(128)S(1)}, u32[]{:S(2)}) copy-start(f32[6]{0:T(128)S(1)} %slice_bitcast_fusion) | copy-start | bytes 76
  155.2 26.6 %copy-start.20 = (s32[192,2]{0,1:T(2,128)S(1)}, s32[192,2]{0,1:T(2,128)}, u32[]{:S(2)}) copy-start(s32[192,2]{0,1:T(2,128)} %param.29) | copy-start | bytes 4612
  155.2 30.5 %copy-start.4 = (bf16[12,1,64,256]{3,2,1,0:T(8,128)(2,1)S(1)}, bf16[12,1,64,256]{3,2,1,0:T(8,128)(2,1)}, u32[]{:S(2)}) copy-start(bf16[12,1,64,256]{3,2,1,0:T(8,128)(2,1)} %get-tuple-element.533) | copy-start | bytes 1179652
  182.1 1.1 copy-start.10
  183.1 0.6 copy-start.14
  183.8 19.9 %copy-start.6 = (s32[96,2]{1,0:T(8,128)}, s32[96,2]{1,0:T(8,128)S(1)}, u32[]{:S(2)}) copy-start(s32[96,2]{1,0:T(8,128)S(1)} %copy.55) | copy-start | bytes 2308
  183.9 19.8 %copy-start.12 = (s32[192]{0:T(256)}, s32[192]{0:T(256)S(1)}, u32[]{:S(2)}) copy-start(s32[192]{0:T(256)S(1)} %eq.114) | copy-start | bytes 2308
  184.9 18.8 %copy-start.16 = (s32[192]{0:T(256)}, s32[192]{0:T(256)S(1)}, u32[]{:S(2)}) copy-start(s32[192]{0:T(256)S(1)} %fusion.98) | copy-start | bytes 2308
  203.8 1.0 copy-start.5
  207.6 5.4 %copy-start.7 = (s32[96,2]{1,0:T(8,128)S(1)}, s32[96,2]{1,0:T(8,128)}, u32[]{:S(2)}) copy-start(s32[96,2]{1,0:T(8,128)} %copy-done.6) | copy-start | bytes 2308
  207.6 5.4 %copy-start.8 = (s32[96,2]{1,0:T(8,128)S(1)}, s32[96,2]{1,0:T(8,128)}, u32[]{:S(2)}) copy-start(s32[96,2]{1,0:T(8,128)} %reduce_sum.106) | copy-start | bytes 2308
  207.6 5.4 %copy-start.9 = (s32[96,2]{1,0:T(8,128)S(1)}, s32[96,2]{1,0:T(8,128)}, u32[]{:S(2)}) copy-start(s32[96,2]{1,0:T(8,128)} %multiply_add_fusion.1) | copy-start | bytes 2308
  209.5 10.8 %all-to-all-start = ((bf16[4,192,256]{2,1,0:T(8,128)(2,1)}), bf16[4,192,256]{2,1,0:T(8,128)(2,1)S(1)}, u32[]{:S(2)}, u32[]{:S(2)}) async-start(bf16[4,192,256]{2,1,0:T(8,128)(2,1)} %bitcast.29), calls=%async_computation | async-start | bytes 786432 | tf_op jit(solution)/shard_map/all_to_all | solution.py:187
  213.4 7.3 %copy-start.24 = (bf16[192,1024]{1,0:T(8,128)(2,1)S(1)}, bf16[192,1024]{1,0:T(8,128)(2,1)}, u32[]{:S(2)}) copy-start(bf16[192,1024]{1,0:T(8,128)(2,1)} %param.23) | copy-start | bytes 1179652
  213.4 7.3 %copy-start.25 = (f32[1024]{0:T(1024)S(1)}, f32[1024]{0:T(1024)}, u32[]{:S(2)}) copy-start(f32[1024]{0:T(1024)} %param.26) | copy-start | bytes 12292
  220.3 1.1 copy-start.23
  221.5 3.5 copy-start.18
  224.9 1.2 copy-start.1
  227.1 104.7 %copy-start.22 = (bf16[1,2048,512]{2,1,0:T(8,128)(2,1)S(1)}, bf16[1,2048,512]{2,1,0:T(8,128)(2,1)}, u32[]{:S(2)}) copy-start(bf16[1,2048,512]{2,1,0:T(8,128)(2,1)} %param.31) | copy-start | bytes 6291460
  330.1 1.7 copy-start.3
  343.0 4.5 %copy-start.11 = (s32[192]{0:T(256)S(1)}, s32[192]{0:T(256)}, u32[]{:S(2)}) copy-start(s32[192]{0:T(256)} %copy-done.10) | copy-start | bytes 2308
  343.0 4.5 %copy-start.15 = (s32[192]{0:T(256)S(1)}, s32[192]{0:T(256)}, u32[]{:S(2)}) copy-start(s32[192]{0:T(256)} %copy-done.14) | copy-start | bytes 2308
  343.0 4.7 %copy-start.13 = (s32[192]{0:T(256)S(1)}, s32[192]{0:T(256)}, u32[]{:S(2)}) copy-start(s32[192]{0:T(256)} %copy-done.12) | copy-start | bytes 2308
  343.0 4.7 %copy-start.17 = (s32[192]{0:T(256)S(1)}, s32[192]{0:T(256)}, u32[]{:S(2)}) copy-start(s32[192]{0:T(256)} %copy-done.16) | copy-start | bytes 2308
  343.0 5.0 %copy-start.19 = (f32[192,2]{0,1:T(2,128)S(1)}, f32[192,2]{0,1:T(2,128)}, u32[]{:S(2)}) copy-start(f32[192,2]{0,1:T(2,128)} %param.30) | copy-start | bytes 4612
  343.0 74.3 %all-to-all-start.2 = ((bf16[8,96,2048]{2,1,0:T(8,128)(2,1)}), bf16[8,96,2048]{2,1,0:T(8,128)(2,1)}, u32[]{:S(2)}, u32[]{:S(2)}) async-start(bf16[8,96,2048]{2,1,0:T(8,128)(2,1)} %convolution_convert_fusion), calls=%async_computation.2 | async-start | bytes 6291456 | tf_op jit(solution)/shard_map/all_to_all | solution.py:235
  420.2 1.4 copy-start.2
Sparse Core Ops, SparseCore 0:
  14.3 51.8 all-gather.4
where the time goes:
time: 436 us; the launch traced here: 430 us
  blocking collectives  143 us (33%)
  matrix products  110 us (25%)
  waiting for transfers between devices  76.2 us (17%)
  other arithmetic  35.8 us (8%)
  local copies, waits for them, and re-layouts  27.3 us (6%)
  loops' own time  15.6 us (4%)
  between operations  14 us (3%)
  starting transfers between devices  7.91 us (2%)
    all_to_all x1, blocking collectives, shards(): lax.all_to_all(send_rows, 'sp', split_axis=0, concat_axis=0, tiled=True)  103 us
    all_to_all x1, waiting for transfers between devices, shards(): lax.all_to_all(finished, 'sp', split_axis=0, concat_axis=0, tiled=True)  69.2 us
    unnamed x1, blocking collectives  23.8 us
    dot_general x12, matrix products, block_step(): jnp.dot(keep_weight, k_float, precision=HIGHEST)  18.9 us
    dot_general x12, matrix products, block_step(): jnp.dot(weights_blk, v_block, preferred_element_type=jnp.float32)  18.9 us
    all_gather x1, blocking collectives, prefix(): gathered = jax.tree.map(lambda a: lax.all_gather(a, axis), part)  16.3 us
    another operation x1, loops' own time, block_pass(): lax.scan(block_step, state, (to_blocks(query), to_blocks(keys), to_blocks...  15.6 us
    dot_general x12, matrix products, block_step(): jnp.dot((k_float * keep_weight[:, None]).T, v_block.astype(jnp.float32),...  15.2 us
  transfers between devices with their start and end apart: 3, of which 2 were waited for; matrix products, arithmetic and copies ran while one was open for 31% of the time, Pallas kernels for 0%

commit v1 on v0

--- a/solution.py
+++ b/solution.py
@@ -7,6 +7,22 @@
 EPS = 1e-06
 FLOOR_LOG = -1e30
 HIGHEST = lax.Precision.HIGHEST
+
+
+def map_rings(field, pos_dim, vec):
+    reply = field.shape
+    top = field.reshape(*reply[:pos_dim], vec, reply[pos_dim] // vec, *reply[pos_dim + 1 :])
+    return jnp.moveaxis(top, pos_dim, 0)
+
+
+def loops_step_on(v0, row_dim):
+    v0 = jnp.moveaxis(v0, 0, row_dim)
+    current_arr = v0.shape
+    return v0.reshape(
+        *current_arr[:row_dim],
+        current_arr[row_dim] * current_arr[row_dim + 1],
+        *current_arr[row_dim + 2 :]
+    )
 
 
 def prefix(part, axis, combine, identity):
@@ -225,12 +241,29 @@
         return packed.astype(jnp.bfloat16).reshape(expert_count, capacity, normed_rows.shape[1])
 
     send_rows = jnp.concatenate([pack_rows(0), pack_rows(1)], axis=1)
+
+    def plan_sites_for(block_here, chip_axis, inner_x, work_x):
+        t_next = jax.lax.axis_size(chip_axis)
+        part_now, k_now = (t_next, jax.lax.axis_index(chip_axis))
+        newest = map_rings(work_x, inner_x, part_now)
+        found = [newest[k_now]]
+        q = 1
+        while q < part_now:
+            base_arr = newest[(k_now + q) % part_now]
+            found.append(
+                jax.lax.ppermute(
+                    base_arr,
+                    axis_name=chip_axis,
+                    perm=[(dev_j, (dev_j + q) % part_now) for dev_j in range(part_now)],
+                )
+            )
+            q = q + 1
+        high = jnp.stack(found, 0)
+        newest = high[(k_now - jnp.arange(part_now)) % part_now]
+        return loops_step_on(newest, block_here)
+
     finished = run_experts(
-        lax.all_to_all(send_rows, "sp", split_axis=0, concat_axis=0, tiled=True),
-        w_gate,
-        w_up,
-        w_down,
-        sources,
+        plan_sites_for(0, "sp", inner_x=0, work_x=send_rows), w_gate, w_up, w_down, sources
     )
     returned = lax.all_to_all(finished, "sp", split_axis=0, concat_axis=0, tiled=True)
     answers = [returned[:, :capacity], returned[:, capacity:]]

time: 436 us -> 443 us (1.016)
  blocking collectives: 143 us -> 40.1 us
  waiting for transfers between devices: 76.2 us -> 128 us
  starting transfers between devices: 7.91 us -> 54.6 us
  local copies, waits for them, and re-layouts: 27.3 us -> 36 us
    all_to_all x1 -> x0, blocking collectives: 103 us -> none  [shards(): lax.all_to_all(send_rows, 'sp', split_axis=0, concat_axis=0, tiled=True)]
    ppermute x0 -> x7, waiting for transfers between devices: none -> 50.3 us  [plan_sites_for(): jax.lax.ppermute(base_arr, axis_name=chip_axis, perm=[(dev_j, (dev_j + q)...]
    ppermute x0 -> x7, starting transfers between devices: none -> 33.5 us  [plan_sites_for(): jax.lax.ppermute(base_arr, axis_name=chip_axis, perm=[(dev_j, (dev_j + q)...]
    all_to_all x1, starting transfers between devices: 4.45 us -> 17.5 us  [shards(): lax.all_to_all(finished, 'sp', split_axis=0, concat_axis=0, tiled=True)]
  transfers between devices with their start and end apart: 3 -> 10, of which waited for: 2 -> 6; matrix products, arithmetic and copies ran while one was open for 31% -> 32% of each run, Pallas kernels for 0% -> 0%
where the time goes in v1:
time: 443 us; the launch traced here: 437 us
  waiting for transfers between devices  128 us (29%)
  matrix products  112 us (25%)
  starting transfers between devices  54.6 us (12%)
  blocking collectives  40.1 us (9%)
  other arithmetic  36.4 us (8%)
  local copies, waits for them, and re-layouts  36 us (8%)
  loops' own time  15.8 us (4%)
  between operations  13.9 us (3%)
    all_to_all x1, waiting for transfers between devices, shards(): lax.all_to_all(finished, 'sp', split_axis=0, concat_axis=0, tiled=True)  70.4 us
    ppermute x7, waiting for transfers between devices, plan_sites_for(): jax.lax.ppermute(base_arr, axis_name=chip_axis, perm=[(dev_j, (dev_j + q)...  50.3 us
    ppermute x7, starting transfers between devices, plan_sites_for(): jax.lax.ppermute(base_arr, axis_name=chip_axis, perm=[(dev_j, (dev_j + q)...  33.5 us
    unnamed x1, blocking collectives  23.8 us
    dot_general x12, matrix products, block_step(): jnp.dot(keep_weight, k_float, precision=HIGHEST)  18.9 us
    dot_general x12, matrix products, block_step(): jnp.dot(weights_blk, v_block, preferred_element_type=jnp.float32)  18.9 us
    all_to_all x1, starting transfers between devices, shards(): lax.all_to_all(finished, 'sp', split_axis=0, concat_axis=0, tiled=True)  17.5 us
    all_gather x1, blocking collectives, prefix(): gathered = jax.tree.map(lambda a: lax.all_gather(a, axis), part)  16.3 us
  transfers between devices with their start and end apart: 10, of which 6 were waited for; matrix products, arithmetic and copies ran while one was open for 32% of the time, Pallas kernels for 0%

profile of v1, /device:TPU:0, one launch (start us, length us, event | category | flops | bytes accessed | tf_op | source)
XLA Modules:
  0.0 436.9 jit_solution(18399473610555001465)
XLA Ops:
  9.2 1.8 fusion.121
  11.6 2.8 fusion.79
  18.4 137.1 %while.38 = (s32[]{:T(128)}, f32[1,256,256]{2,1,0:T(8,128)S(1)}, f32[1,256]{1,0:T(1,128)S(1)}, f32[1]{0:T(128)}, f32[12,1,64,256]{3,2,1,0:T(8,128)}, /*index=5*/...) while((s32[]{:T(128)}, f32[1,256,256]{2,1,0:T(8,128)S(1)}, ...), condition=%wide.region_5.6_spmd.clone, body=%wide.region_0.5_spmd.clone.sunk | while | flops 105678720 | bytes 1284879 | solution.py:82
  24.4 1.6 convolution_add_fusion.4
  28.2 1.6 fusion.168
  35.8 1.6 convolution_add_fusion.4
  39.7 1.6 fusion.168
  47.3 1.6 convolution_add_fusion.4
  51.1 1.6 fusion.168
  58.7 1.6 convolution_add_fusion.4
  62.5 1.6 fusion.168
  70.1 1.6 convolution_add_fusion.4
  81.5 1.6 convolution_add_fusion.4
  85.4 1.6 fusion.168
  155.5 23.8 %all-reduce.4 = (f32[8]{0:T(128)}, f32[8]{0:T(128)}) all-reduce(f32[8]{0:T(128)S(1)} %bitcast_dynamic-update-slice_fusion.8, f32[8]{0:T(128)S(1)} %dynamic-update-slice.1), channel_id=1, replica_groups=mesh['sp'=8,'tp'=4] {'sp'}, use_global_device_ids=true, to_apply=%add.2 | all-reduce | flops 16 | bytes 128
  188.5 16.3 %all-gather.2 = f32[8,1,256]{2,1,0:T(1,128)S(1)} all-gather(f32[1,1,256]{2,1,0:T(1,128)S(1)} %convolution_bitcast_fusion.3), channel_id=3, replica_groups=mesh['sp'=8,'tp'=4] {'sp'}, dimensions={0}, use_global_device_ids=true | all-gather | bytes 9216 | tf_op jit(solution)/shard_map/all_gather | solution.py:30
  209.2 1.9 copy.46
  211.1 3.6 all-to-all-start
  215.0 7.1 %all-to-all-done = bf16[4,192,256]{2,1,0:T(8,128)(2,1)S(1)} async-done(((bf16[4,192,256]{2,1,0:T(8,128)(2,1)}), bf16[4,192,256]{2,1,0:T(8,128)(2,1)S(1)}, u32[]{:S(2)}, u32[]{:S(2)}) %all-to-all-start) | async-done | bytes 393248 | tf_op jit(solution)/shard_map/all_to_all | solution.py:203
  223.1 3.5 multiply_reduce_fusion
  228.6 5.5 %collective-permute-start = (bf16[1,96,2048]{2,1,0:T(8,128)(2,1)S(1)}, bf16[1,96,2048]{2,1,0:T(8,128)(2,1)S(1)}, u32[]{:S(2)}, u32[]{:S(2)}) collective-permute-start(bf16[1,96,2048]{2,1,0:T(8,128)(2,1)S(1)} %get-tuple-element.296), channel_id=1, source_target_pairs={{0,4},{4,8},{8,12},{12,16},{16,20},{20,24},{24,28},{28,0},{1,5},{5... | collective-permute-start | bytes 1179656 | tf_op jit(solution)/shard_map/ppermute | solution.py:254
  234.1 26.5 %collective-permute-start.5 = (bf16[1,96,2048]{2,1,0:T(8,128)(2,1)S(1)}, bf16[1,96,2048]{2,1,0:T(8,128)(2,1)S(1)}, u32[]{:S(2)}, u32[]{:S(2)}) collective-permute-start(bf16[1,96,2048]{2,1,0:T(8,128)(2,1)S(1)} %fusion.90), channel_id=1, source_target_pairs={{0,24},{4,28},{8,0},{12,4},{16,8},{20,12},{24,16},{28,20},{1,25},{... | collective-permute-start | bytes 1179656 | tf_op jit(solution)/shard_map/ppermute | solution.py:254
  262.9 7.1 %collective-permute-done = bf16[1,96,2048]{2,1,0:T(8,128)(2,1)S(1)} collective-permute-done((bf16[1,96,2048]{2,1,0:T(8,128)(2,1)S(1)}, bf16[1,96,2048]{2,1,0:T(8,128)(2,1)S(1)}, u32[]{:S(2)}, u32[]{:S(2)}) %collective-permute-start) | collective-permute-done | bytes 393248 | tf_op jit(solution)/shard_map/ppermute | solution.py:254
  270.7 16.8 %collective-permute-done.1 = bf16[1,96,2048]{2,1,0:T(8,128)(2,1)S(1)} collective-permute-done((bf16[1,96,2048]{2,1,0:T(8,128)(2,1)S(1)}, bf16[1,96,2048]{2,1,0:T(8,128)(2,1)S(1)}, u32[]{:S(2)}, u32[]{:S(2)}) %collective-permute-start.1) | collective-permute-done | bytes 393248 | tf_op jit(solution)/shard_map/ppermute | solution.py:254
  288.3 19.3 %collective-permute-done.2 = bf16[1,96,2048]{2,1,0:T(8,128)(2,1)S(1)} collective-permute-done((bf16[1,96,2048]{2,1,0:T(8,128)(2,1)S(1)}, bf16[1,96,2048]{2,1,0:T(8,128)(2,1)S(1)}, u32[]{:S(2)}, u32[]{:S(2)}) %collective-permute-start.2) | collective-permute-done | bytes 393248 | tf_op jit(solution)/shard_map/ppermute | solution.py:254
  308.4 7.2 %collective-permute-done.3 = bf16[1,96,2048]{2,1,0:T(8,128)(2,1)S(1)} collective-permute-done((bf16[1,96,2048]{2,1,0:T(8,128)(2,1)S(1)}, bf16[1,96,2048]{2,1,0:T(8,128)(2,1)S(1)}, u32[]{:S(2)}, u32[]{:S(2)}) %collective-permute-start.3) | collective-permute-done | bytes 393248 | tf_op jit(solution)/shard_map/ppermute | solution.py:254
  318.7 4.3 gather_fusion
  323.0 5.6 %fusion.60 = f32[8,96,512]{2,1,0:T(8,128)} fusion(bf16[8,96,2048]{2,1,0:T(8,128)(2,1)} %gather_fusion, bf16[1,2048,512]{2,1,0:T(8,128)(2,1)} %param.31), kind=kOutput, calls=%fused_computation.104 | convolution fusion | flops 1610612736 | bytes 6815744 | tf_op jit(solution)/shard_map/pesd,edf->pesf/dot_general | solution.py:142
  328.6 8.2 %convolution_convert_fusion = bf16[8,96,2048]{2,1,0:T(8,128)(2,1)} fusion(bf16[1,512,2048]{2,1,0:T(8,128)(2,1)S(1)} %copy-done, bf16[8,96,2048]{2,1,0:T(8,128)(2,1)} %gather_fusion, bf16[1,2048,512]{2,1,0:T(8,128)(2,1)} %param.32, f32[8,96,512]{2,1,0:T(8,128)} %fusion.60), kind=kOutput, calls=%fused_computation.95 | convolution fusion | flops 3225157632 | bytes 12058624 | tf_op jit(solution)/shard_map/pesf,efd->pesd/dot_general | solution.py:145
  336.8 17.5 %all-to-all-start.1 = ((bf16[8,96,2048]{2,1,0:T(8,128)(2,1)}), bf16[8,96,2048]{2,1,0:T(8,128)(2,1)}, u32[]{:S(2)}, u32[]{:S(2)}) async-start(bf16[8,96,2048]{2,1,0:T(8,128)(2,1)} %convolution_convert_fusion), calls=%async_computation.1 | async-start | bytes 6291456 | tf_op jit(solution)/shard_map/all_to_all | solution.py:268
  354.9 70.4 %all-to-all-done.1 = bf16[8,96,2048]{2,1,0:T(8,128)(2,1)} async-done(((bf16[8,96,2048]{2,1,0:T(8,128)(2,1)}), bf16[8,96,2048]{2,1,0:T(8,128)(2,1)}, u32[]{:S(2)}, u32[]{:S(2)}) %all-to-all-start.1) | async-done | bytes 3145760 | tf_op jit(solution)/shard_map/all_to_all | solution.py:268
  425.3 2.3 fusion.122
  (309 shorter events, 138.4 us)
Async XLA Ops:
  6.5 322.1 %copy-start = (bf16[1,512,2048]{2,1,0:T(8,128)(2,1)S(1)}, bf16[1,512,2048]{2,1,0:T(8,128)(2,1)}, u32[]{:S(2)}) copy-start(bf16[1,512,2048]{2,1,0:T(8,128)(2,1)} %param.33) | copy-start | bytes 6291460
  6.5 198.8 %all-gather.5.cloned.1.call-start = ((), (), s32[]{:S(2)}) async-start(), calls=%async_computation.2 | async-start | bytes 2359296 | tf_op jit(solution)/shard_map/all_gather | solution.py:30
  18.4 161.0 %copy-start.17 = (s32[192,2]{0,1:T(2,128)S(1)}, s32[192,2]{0,1:T(2,128)}, u32[]{:S(2)}) copy-start(s32[192,2]{0,1:T(2,128)} %param.29) | copy-start | bytes 4612
  155.5 32.0 %copy-start.3 = (bf16[12,1,64,256]{3,2,1,0:T(8,128)(2,1)S(1)}, bf16[12,1,64,256]{3,2,1,0:T(8,128)(2,1)}, u32[]{:S(2)}) copy-start(bf16[12,1,64,256]{3,2,1,0:T(8,128)(2,1)} %get-tuple-element.539) | copy-start | bytes 1179652
  179.7 1.0 copy-start.5
  180.7 0.6 copy-start.9
  182.3 1.0 copy-start.7
  183.3 0.6 copy-start.11
  205.4 1.0 copy-start.4
  207.6 7.1 %copy-start.19 = (s32[8]{0:T(128)S(1)}, s32[8]{0:T(128)}, u32[]{:S(2)}) copy-start(s32[8]{0:T(128)} %fusion.116) | copy-start | bytes 100
  207.6 7.1 %copy-start.16 = (s32[96,2]{0,1:T(2,128)S(1)}, s32[96,2]{0,1:T(2,128)}, u32[]{:S(2)}) copy-start(s32[96,2]{0,1:T(2,128)} %copy.51) | copy-start | bytes 2308
  207.6 7.2 %copy-start.15 = (s32[96,2]{0,1:T(2,128)S(1)}, s32[96,2]{0,1:T(2,128)}, u32[]{:S(2)}) copy-start(s32[96,2]{0,1:T(2,128)} %copy.49) | copy-start | bytes 2308
  211.1 11.3 %copy-start.20 = (bf16[192,2048]{1,0:T(8,128)(2,1)S(1)}, bf16[192,2048]{1,0:T(8,128)(2,1)}, u32[]{:S(2)}) copy-start(bf16[192,2048]{1,0:T(8,128)(2,1)} %param.19) | copy-start | bytes 2359300
  211.1 11.3 %copy-start.22 = (f32[1024]{0:T(1024)S(1)}, f32[1024]{0:T(1024)}, u32[]{:S(2)}) copy-start(f32[1024]{0:T(1024)} %param.26) | copy-start | bytes 12292
  211.1 11.0 %all-to-all-start = ((bf16[4,192,256]{2,1,0:T(8,128)(2,1)}), bf16[4,192,256]{2,1,0:T(8,128)(2,1)S(1)}, u32[]{:S(2)}, u32[]{:S(2)}) async-start(bf16[4,192,256]{2,1,0:T(8,128)(2,1)} %bitcast.29), calls=%async_computation | async-start | bytes 786432 | tf_op jit(solution)/shard_map/all_to_all | solution.py:203
  222.1 1.0 copy-start.21
  223.1 3.5 copy-start.13
  226.6 1.2 copy-start.1
  228.6 41.3 %collective-permute-start = (bf16[1,96,2048]{2,1,0:T(8,128)(2,1)S(1)}, bf16[1,96,2048]{2,1,0:T(8,128)(2,1)S(1)}, u32[]{:S(2)}, u32[]{:S(2)}) collective-permute-start(bf16[1,96,2048]{2,1,0:T(8,128)(2,1)S(1)} %get-tuple-element.296), channel_id=1, source_target_pairs={{0,4},{4,8},{8,12},{12,16},{16,20},{20,24},{24,28},{28,0},{1,5},{5... | collective-permute-start | bytes 1179656 | tf_op jit(solution)/shard_map/ppermute | solution.py:254
  234.1 83.0 %collective-permute-start.5 = (bf16[1,96,2048]{2,1,0:T(8,128)(2,1)S(1)}, bf16[1,96,2048]{2,1,0:T(8,128)(2,1)S(1)}, u32[]{:S(2)}, u32[]{:S(2)}) collective-permute-start(bf16[1,96,2048]{2,1,0:T(8,128)(2,1)S(1)} %fusion.90), channel_id=1, source_target_pairs={{0,24},{4,28},{8,0},{12,4},{16,8},{20,12},{24,16},{28,20},{1,25},{... | collective-permute-start | bytes 1179656 | tf_op jit(solution)/shard_map/ppermute | solution.py:254
  260.6 57.3 %collective-permute-start.6 = (bf16[1,96,2048]{2,1,0:T(8,128)(2,1)S(1)}, bf16[1,96,2048]{2,1,0:T(8,128)(2,1)S(1)}, u32[]{:S(2)}, u32[]{:S(2)}) collective-permute-start(bf16[1,96,2048]{2,1,0:T(8,128)(2,1)S(1)} %get-tuple-element.295), channel_id=1, source_target_pairs={{0,28},{4,0},{8,4},{12,8},{16,12},{20,16},{24,20},{28,24},{1,29},{... | collective-permute-start | bytes 1179656 | tf_op jit(solution)/shard_map/ppermute | solution.py:254
  260.6 26.9 %collective-permute-start.1 = (bf16[1,96,2048]{2,1,0:T(8,128)(2,1)S(1)}, bf16[1,96,2048]{2,1,0:T(8,128)(2,1)S(1)}, u32[]{:S(2)}, u32[]{:S(2)}) collective-permute-start(bf16[1,96,2048]{2,1,0:T(8,128)(2,1)S(1)} %get-tuple-element.297), channel_id=1, source_target_pairs={{0,8},{4,12},{8,16},{12,20},{16,24},{20,28},{24,0},{28,4},{1,9},{5... | collective-permute-start | bytes 1179656 | tf_op jit(solution)/shard_map/ppermute | solution.py:254
  262.1 45.5 %collective-permute-start.2 = (bf16[1,96,2048]{2,1,0:T(8,128)(2,1)S(1)}, bf16[1,96,2048]{2,1,0:T(8,128)(2,1)S(1)}, u32[]{:S(2)}, u32[]{:S(2)}) collective-permute-start(bf16[1,96,2048]{2,1,0:T(8,128)(2,1)S(1)} %get-tuple-element.298), channel_id=1, source_target_pairs={{0,12},{4,16},{8,20},{12,24},{16,28},{20,0},{24,4},{28,8},{1,13},{... | collective-permute-start | bytes 1179656 | tf_op jit(solution)/shard_map/ppermute | solution.py:254
  269.9 45.6 %collective-permute-start.3 = (bf16[1,96,2048]{2,1,0:T(8,128)(2,1)S(1)}, bf16[1,96,2048]{2,1,0:T(8,128)(2,1)S(1)}, u32[]{:S(2)}, u32[]{:S(2)}) collective-permute-start(bf16[1,96,2048]{2,1,0:T(8,128)(2,1)S(1)} %get-tuple-element.299), channel_id=1, source_target_pairs={{0,16},{4,20},{8,24},{12,28},{16,0},{20,4},{24,8},{28,12},{1,17},{... | collective-permute-start | bytes 1179656 | tf_op jit(solution)/shard_map/ppermute | solution.py:254
  287.5 28.8 %collective-permute-start.4 = (bf16[1,96,2048]{2,1,0:T(8,128)(2,1)S(1)}, bf16[1,96,2048]{2,1,0:T(8,128)(2,1)S(1)}, u32[]{:S(2)}, u32[]{:S(2)}) collective-permute-start(bf16[1,96,2048]{2,1,0:T(8,128)(2,1)S(1)} %get-tuple-element.300), channel_id=1, source_target_pairs={{0,20},{4,24},{8,28},{12,0},{16,4},{20,8},{24,12},{28,16},{1,21},{... | collective-permute-start | bytes 1179656 | tf_op jit(solution)/shard_map/ppermute | solution.py:254
  336.8 17.6 %copy-start.6 = (s32[192]{0:T(256)S(1)}, s32[192]{0:T(256)}, u32[]{:S(2)}) copy-start(s32[192]{0:T(256)} %copy-done.5) | copy-start | bytes 2308
  336.8 17.6 %copy-start.10 = (s32[192]{0:T(256)S(1)}, s32[192]{0:T(256)}, u32[]{:S(2)}) copy-start(s32[192]{0:T(256)} %copy-done.9) | copy-start | bytes 2308
  336.8 17.8 %copy-start.8 = (s32[192]{0:T(256)S(1)}, s32[192]{0:T(256)}, u32[]{:S(2)}) copy-start(s32[192]{0:T(256)} %copy-done.7) | copy-start | bytes 2308
  336.8 17.8 %copy-start.12 = (s32[192]{0:T(256)S(1)}, s32[192]{0:T(256)}, u32[]{:S(2)}) copy-start(s32[192]{0:T(256)} %copy-done.11) | copy-start | bytes 2308
  336.8 18.0 %copy-start.14 = (f32[192,2]{0,1:T(2,128)S(1)}, f32[192,2]{0,1:T(2,128)}, u32[]{:S(2)}) copy-start(f32[192,2]{0,1:T(2,128)} %param.30) | copy-start | bytes 4612
  336.8 88.5 %all-to-all-start.1 = ((bf16[8,96,2048]{2,1,0:T(8,128)(2,1)}), bf16[8,96,2048]{2,1,0:T(8,128)(2,1)}, u32[]{:S(2)}, u32[]{:S(2)}) async-start(bf16[8,96,2048]{2,1,0:T(8,128)(2,1)} %convolution_convert_fusion), calls=%async_computation.1 | async-start | bytes 6291456 | tf_op jit(solution)/shard_map/all_to_all | solution.py:268
  427.6 1.4 copy-start.2
  (1 other events, 0.5 us)
Sparse Core Ops, SparseCore 0:
  14.5 52.1 all-gather.4
